TPU v7x, 32 devices: a whole 2x2x4 slice. The times are simulated.
32 devices in a mesh: sp: 8 (over z, y), tp: 4 (over x, core).
Axes of the slice: x: 2, y: 2, z: 4, core: 2. Of those that a mesh axis runs over, the one named last changes fastest.
Arguments:
- queries: bfloat16 [4096, 1024], P('sp', 'tp'), may hold values from -6 to 6
- keys: bfloat16 [4096, 1024], P('sp', 'tp'), may hold values from -6 to 6
- values: bfloat16 [4096, 1024], P('sp', 'tp'), may hold values from -12 to 12
- breaks: bfloat16 [4096, 8], P('sp', 'tp'), may hold values from -12 to 0.5
- residual_in: bfloat16 [4096, 2048], P('sp', 'tp'), may hold values from -6 to 6
- out_weight: bfloat16 [1024, 2048], P('tp'), may hold values from -0.1875 to 0.1875
- first_gain: float32 [2048], replicated, may hold values from 0.1 to 1.9
- first_shift: float32 [2048], replicated, may hold values from -2 to 2
- up_weight: bfloat16 [2048, 8192], P('sp', 'tp'), may hold values from -0.125 to 0.125
- down_weight: bfloat16 [2048, 8192], P('sp', 'tp'), may hold values from -0.0625 to 0.0625
- second_gain: float32 [2048], replicated, may hold values from 0.1 to 1.9
- second_shift: float32 [2048], replicated, may hold values from -2 to 2
Outputs:
- layer_out: bfloat16 [4096, 2048], P('sp', 'tp')
All inputs are finite; a program needn't handle non-finite values.
Results may differ from a plain program's by a relative error of at most 0.018.
Values may be sent and summed in bfloat16 or wider, within the bound.
A program may use at most 128 MiB of HBM per device.

v0:
```python
import functools

import jax
import jax.numpy as jnp
from jax import lax
from jax.experimental import pallas as pl
from jax.experimental.pallas import tpu as pltpu
from jax.sharding import PartitionSpec as P

ALPHA = 2.0**0.25
EPSILON = 1e-05
MESH = pl.DeviceIdType.MESH
F32 = jnp.float32
BF16 = jnp.bfloat16
KV, UP, DOWN = 0, 1, 2
RIGHT, LEFT = 0, 1


def aligned(start, size):
    return pl.ds(pl.multiple_of(start, size), size)


def layer_kernel(
    n,
    t,
    heads,
    q_ref,
    kv_in,
    br_in,
    res_in,
    ow_in,
    g1_ref,
    b1_ref,
    up_in,
    down_in,
    g2_ref,
    b2_ref,
    out_ref,
    kv,
    up,
    down,
    br,
    ow,
    res,
    later_sum,
    totals,
    att_all,
    lower,
    pre,
    first,
    activated,
    part,
    mix,
    stat,
    ring_send,
    ring_recv,
    br_send,
    br_recv,
    ow_send,
    ow_recv,
    res_send,
    res_recv,
    att_send,
    att_recv,
    mix_send,
    mix_recv,
    stat_send,
    stat_recv,
    local_sem,
):
    me = lax.axis_index("sp")
    me_t = lax.axis_index("tp")
    tok = q_ref.shape[0]
    width = q_ref.shape[1]
    hd = width // heads
    feat = first.shape[1]
    cols = feat // t
    block = feat // n
    per = n // t
    half_n = n // 2

    def at_pos(p):
        p = lax.rem(p + n, n)
        back = p // half_n
        return 2 * (p + back * (n - 1 - 2 * p)) + back

    pos = me // 2 + lax.rem(me, 2) * (n - 1 - 2 * (me // 2))
    next_dev = (at_pos(pos + 1), at_pos(pos - 1))
    own_in = (kv_in, up_in, down_in)
    full = (kv, up, down)
    rows_of = (tok, block, block)

    def ring_copy(item, way, hop, piece, own=False):
        rows = rows_of[item]
        half = rows // 2
        owner = at_pos(pos - (hop - 1) if way == RIGHT else pos + (hop - 1))
        dst = full[item].at[aligned(owner * rows + piece * half, half)]
        src = own_in[item].at[aligned(piece * half, half)] if own else dst
        return pltpu.make_async_remote_copy(
            src_ref=src,
            dst_ref=dst,
            send_sem=ring_send.at[item, way, hop, piece],
            recv_sem=ring_recv.at[item, way, hop, piece],
            device_id={"sp": next_dev[way]},
            device_id_type=MESH,
        )

    def ring_landed(item, way, hop, piece):
        rows = rows_of[item]
        half = rows // 2
        owner = at_pos(pos - hop if way == RIGHT else pos + hop)
        dst = full[item].at[aligned(owner * rows + piece * half, half)]
        return pltpu.make_async_remote_copy(
            src_ref=dst,
            dst_ref=dst,
            send_sem=ring_send.at[item, way, hop, piece],
            recv_sem=ring_recv.at[item, way, hop, piece],
            device_id={"sp": next_dev[way]},
            device_id_type=MESH,
        )

    def start_own(item):
        ring_copy(item, RIGHT, 1, 0, own=True).start()
        ring_copy(item, LEFT, 1, 1, own=True).start()
        ring_copy(item, RIGHT, 1, 1, own=True).start()
        ring_copy(item, LEFT, 1, 0, own=True).start()

    def event(item, e, hop=None, second=None):
        static = isinstance(e, int)
        hop = 1 + e // 2
        second = e % 2 if static else lax.rem(e, 2)
        ring_landed(item, RIGHT, hop, second).wait_recv()

        def forward_right():
            ring_copy(item, RIGHT, hop + 1, second).start()

        def forward_left():
            ring_copy(item, LEFT, hop + 1, 1 - second).start()

        def start_next():
            if item < DOWN:
                start_own(item + 1)

        def guarded(cond, fn):
            if static:
                if cond:
                    fn()
            else:
                pl.when(cond)(fn)

        guarded(e < n - 3, forward_right)
        ring_landed(item, LEFT, hop, 1 - second).wait_recv()
        guarded(e < n - 3, forward_left)
        guarded(e == n - 4, start_next)

    def drain_sends(item):
        def one(e, _):
            hop = 1 + e // 2
            second = lax.rem(e, 2)
            ring_copy(item, RIGHT, hop, second).wait_send()
            ring_copy(item, LEFT, hop, 1 - second).wait_send()
            return 0

        lax.fori_loop(0, n - 1, one, 0)

    def peer_t(d):
        return lax.rem(me_t + d, t)

    def tp_copy(src, dst_of, sends, recvs, d):
        return pltpu.make_async_remote_copy(
            src_ref=src,
            dst_ref=dst_of(me_t),
            send_sem=sends.at[d],
            recv_sem=recvs.at[d],
            device_id={"tp": peer_t(d)},
            device_id_type=MESH,
        )

    def tp_landed(dst_of, sends, recvs, d):
        dst = dst_of(lax.rem(me_t + t - d, t))
        return pltpu.make_async_remote_copy(
            src_ref=dst,
            dst_ref=dst,
            send_sem=sends.at[d],
            recv_sem=recvs.at[d],
            device_id={"tp": peer_t(d)},
            device_id_type=MESH,
        )

    def br_copy(d, landed=False):
        owner = lax.rem(me + n - d, n) if landed else me
        return pltpu.make_async_remote_copy(
            src_ref=br.at[owner] if landed else br_in,
            dst_ref=br.at[owner],
            send_sem=br_send.at[d],
            recv_sem=br_recv.at[d],
            device_id={"sp": lax.rem(me + d, n)},
            device_id_type=MESH,
        )

    barrier = pltpu.get_barrier_semaphore()

    def greet(d, _):
        pl.semaphore_signal(
            barrier, inc=1, device_id={"sp": lax.rem(me + d, n)}, device_id_type=MESH
        )
        return 0

    lax.fori_loop(1, n, greet, 0)
    for d in range(1, t):
        pl.semaphore_signal(barrier, inc=1, device_id={"tp": peer_t(d)}, device_id_type=MESH)

    res_at = lambda g: res.at[g]
    ow_at = lambda g: ow.at[g]
    att_at = lambda g: att_all.at[g]

    locals_ = [
        pltpu.make_async_copy(kv_in, kv.at[aligned(me * tok, tok)], local_sem.at[0]),
        pltpu.make_async_copy(up_in, up.at[aligned(me * block, block)], local_sem.at[1]),
        pltpu.make_async_copy(down_in, down.at[aligned(me * block, block)], local_sem.at[2]),
        pltpu.make_async_copy(br_in, br.at[me], local_sem.at[3]),
        pltpu.make_async_copy(res_in, res.at[me_t], local_sem.at[4]),
        pltpu.make_async_copy(ow_in, ow.at[me_t], local_sem.at[5]),
    ]
    pl.semaphore_wait(barrier, n - 1 + t - 1)
    start_own(KV)

    def send_breaks(d, _):
        br_copy(d).start()
        return 0

    lax.fori_loop(1, n, send_breaks, 0)
    for c in locals_:
        c.start()
    for d in range(1, t):
        tp_copy(ow_in, ow_at, ow_send, ow_recv, d).start()
    for d in range(1, t):
        tp_copy(res_in, res_at, res_send, res_recv, d).start()

    key_row = lax.broadcasted_iota(jnp.int32, (tok, tok), 0)
    key_col = lax.broadcasted_iota(jnp.int32, (tok, tok), 1)
    lower[...] = jnp.where(key_row > key_col, 1.0, 0.0).astype(BF16)
    later_sum[...] = jnp.zeros_like(later_sum)
    totals[...] = jnp.zeros_like(totals)

    def kv_event(e, _):
        event(KV, e)
        return 0

    lax.fori_loop(0, n - 2, kv_event, 0)

    def last_event(item):
        ring_landed(item, RIGHT, half_n, 0).wait_recv()
        ring_landed(item, LEFT, half_n, 1).wait_recv()

    last_event(KV)

    def wait_breaks(d, _):
        br_copy(d, landed=True).wait_recv()
        return 0

    lax.fori_loop(1, n, wait_breaks, 0)
    for c in locals_:
        c.wait()

    scale = hd ** (-0.5)
    tile = 128

    def attend_block(j):
        b = me - j
        for h in range(heads):
            def rows(i, _):
                at = aligned(i * tile, tile)
                keys = kv[aligned(b * tok, tok), pl.ds(h * hd, hd)]
                vals = kv[aligned(b * tok, tok), pl.ds(width + h * hd, hd)]
                z = lax.dot_general(
                    q_ref[at, pl.ds(h * hd, hd)],
                    keys,
                    (((1,), (1,)), ((), ())),
                    preferred_element_type=F32,
                )
                z = z * scale + br[b, pl.ds(h, 1), :]
                soft = jnp.log(1.0 + jnp.exp(-jnp.abs(z)))
                log_break = jnp.minimum(z, 0.0) - soft
                r = lax.broadcasted_iota(jnp.int32, (tile, tok), 0) + i * tile + j * tok
                strict = lax.broadcasted_iota(jnp.int32, (tile, tok), 1) < r
                log_keep = jnp.where(strict, log_break - z, 0.0)
                high = log_keep.astype(BF16)
                low = (log_keep - high.astype(F32)).astype(BF16)
                tri = lower[...]
                later = jnp.dot(high, tri, preferred_element_type=F32) + jnp.dot(
                    low, tri, preferred_element_type=F32
                )
                before = later_sum[h, at, :]
                w = jnp.exp(log_break + later + before[:, 0:1])
                w = jnp.where(strict, w, 0.0).astype(BF16)
                totals[at, pl.ds(h * hd, hd)] += jnp.dot(w, vals, preferred_element_type=F32)
                later_sum[h, at, :] = before + jnp.sum(log_keep, axis=1, keepdims=True)
                return 0

            lax.fori_loop(0, tok // tile, rows, 0)

    def attend_step(j, _):
        @pl.when(j <= me)
        def _():
            attend_block(j)

        @pl.when(j < n - 2)
        def _():
            event(UP, j)

        return 0

    lax.fori_loop(0, n, attend_step, 0)

    own_att = att_all.at[me_t]
    own_att[...] = totals[...].astype(BF16)
    for d in range(1, t):
        tp_copy(own_att, att_at, att_send, att_recv, d).start()
    last_event(UP)
    for d in range(1, t):
        tp_landed(ow_at, ow_send, ow_recv, d).wait_recv()
        tp_landed(res_at, res_send, res_recv, d).wait_recv()
    for d in range(1, t):
        tp_landed(att_at, att_send, att_recv, d).wait_recv()

    big = 256

    def mix_rows(i, _):
        at = aligned(i * big, big)
        for c in range(t):
            lanes = pl.ds(c * cols, cols)
            acc = ALPHA * res[c, at, :].astype(F32)
            mixed = jnp.zeros((big, cols), F32)
            for g in range(t):
                mixed = mixed + jnp.dot(
                    att_all[g, at, :], ow[g, :, lanes], preferred_element_type=F32
                ).astype(BF16).astype(F32)
            pre[at, lanes] = acc + mixed
        return 0

    lax.fori_loop(0, tok // big, mix_rows, 0)
    event(DOWN, 0)

    small = 64

    def norm_rows(i, _):
        at = aligned(i * small, small)
        x = pre[at, :]
        center = jnp.sum(x, axis=1, keepdims=True) / feat
        x = x - center
        spread = jnp.sum(x * x, axis=1, keepdims=True) / feat
        first[at, :] = (x * lax.rsqrt(spread + EPSILON) * g1_ref[...] + b1_ref[...]).astype(BF16)
        return 0

    lax.fori_loop(0, tok // small, norm_rows, 0)

    hidden = up.shape[1]
    strip = 256

    def up_cols(i, _):
        lanes = aligned(i * strip, strip)
        a = jnp.dot(first[...], up[:, lanes], preferred_element_type=F32)
        a = jnp.maximum(a, 0.0)
        activated[:, lanes] = (a * a).astype(BF16)
        return 0

    event(DOWN, 1)
    lax.fori_loop(0, hidden // strip, up_cols, 0)

    def mix_copy(s):
        k = lax.rem(s, per)
        owner = s // per
        return owner, pltpu.make_async_remote_copy(
            src_ref=part.at[s],
            dst_ref=mix.at[me_t, k],
            send_sem=mix_send.at[s],
            recv_sem=mix_recv.at[me_t, k],
            device_id={"tp": owner},
            device_id_type=MESH,
        )

    def down_block(s):
        y = lax.dot_general(
            activated[...],
            down[aligned(s * block, block), :],
            (((1,), (1,)), ((), ())),
            preferred_element_type=F32,
        ).astype(BF16)
        owner, copy = mix_copy(s)

        @pl.when(owner == me_t)
        def _():
            mix[me_t, lax.rem(s, per)] = y

        @pl.when(owner != me_t)
        def _():
            part[s] = y
            copy.start()

    down_block(me)

    def down_step(h, _):
        @pl.when(h > 1)
        def _():
            event(DOWN, 2 * h - 2)
            event(DOWN, 2 * h - 1)

        def side(w, _):
            down_block(at_pos(pos + (2 * w - 1) * h))
            return 0

        lax.fori_loop(0, 2, side, 0)
        return 0

    lax.fori_loop(1, half_n, down_step, 0)
    last_event(DOWN)
    down_block(at_pos(pos + half_n))

    def mix_wait(s, _):
        owner, copy = mix_copy(s)

        @pl.when(owner != me_t)
        def _():
            copy.wait_send()

        return 0

    for d in range(1, t):
        g = lax.rem(me_t + t - d, t)
        for k in range(per):
            dst = mix.at[g, k]
            pltpu.make_async_remote_copy(
                src_ref=dst,
                dst_ref=dst,
                send_sem=mix_send.at[0],
                recv_sem=mix_recv.at[g, k],
                device_id={"tp": peer_t(d)},
                device_id_type=MESH,
            ).wait_recv()

    def second_pre(i, _):
        at = aligned(i * 128, 128)
        sums = jnp.zeros((128, 1), F32)
        squares = jnp.zeros((128, 1), F32)
        x = ALPHA * first[at, aligned(me_t * cols, cols)].astype(F32)
        pieces = []
        for k in range(per):
            v = mix[0, k, at, :].astype(F32)
            for g in range(1, t):
                v = v + mix[g, k, at, :].astype(F32)
            pieces.append(v)
        x = x + (jnp.concatenate(pieces, axis=1) if per > 1 else pieces[0])
        pre[at, pl.ds(0, cols)] = x
        sums = jnp.sum(x, axis=1, keepdims=True)
        squares = jnp.sum(x * x, axis=1, keepdims=True)
        lane = lax.broadcasted_iota(jnp.int32, (128, 128), 1)
        s = jnp.where(lane == 0, sums, jnp.where(lane == 1, squares, 0.0))
        stat[me_t, :, at] = s.T[0:8, :]
        return 0

    for i in range(tok // 128):
        second_pre(i, 0)
    stat_at = lambda g: stat.at[g]
    for d in range(1, t):
        tp_copy(stat.at[me_t], stat_at, stat_send, stat_recv, d).start()

    lax.fori_loop(0, n, mix_wait, 0)
    for item in (KV, UP, DOWN):
        drain_sends(item)

    def br_done(d, _):
        br_copy(d).wait_send()
        return 0

    lax.fori_loop(1, n, br_done, 0)
    for d in range(1, t):
        tp_copy(ow_in, ow_at, ow_send, ow_recv, d).wait_send()
        tp_copy(res_in, res_at, res_send, res_recv, d).wait_send()
        tp_copy(own_att, att_at, att_send, att_recv, d).wait_send()
    for d in range(1, t):
        tp_landed(stat_at, stat_send, stat_recv, d).wait_recv()

    for i in range(tok // 128):
        at = pl.ds(i * 128, 128)
        s = stat[0, :, at]
        for g in range(1, t):
            s = s + stat[g, :, at]
        s = jnp.concatenate([s, jnp.zeros((120, 128), F32)], axis=0).T
        center = s[:, 0:1] / feat
        spread = s[:, 1:2] / feat - center * center
        x = pre[at, pl.ds(0, cols)]
        x = (x - center) * lax.rsqrt(spread + EPSILON)
        out_ref[at, :] = (x * g2_ref[me_t] + b2_ref[me_t]).astype(BF16)
    for d in range(1, t):
        tp_copy(stat.at[me_t], stat_at, stat_send, stat_recv, d).wait_send()


def solution(mesh):
    n, t = mesh.shape["sp"], mesh.shape["tp"]

    def body(
        queries,
        keys,
        values,
        breaks,
        residual_in,
        out_weight,
        first_gain,
        first_shift,
        up_weight,
        down_weight,
        second_gain,
        second_shift,
    ):
        tok, width = queries.shape
        heads = breaks.shape[1]
        feat = out_weight.shape[1]
        cols = residual_in.shape[1]
        hidden = up_weight.shape[1]
        block = up_weight.shape[0]
        per = n // t
        kv = jnp.concatenate([keys, values], axis=1)
        br = jnp.pad(breaks.astype(F32).T, ((0, 8 - heads), (0, 0)))
        any_ = pl.BlockSpec(memory_space=pl.ANY)
        vmem = pl.BlockSpec(memory_space=pltpu.VMEM)
        dma = pltpu.SemaphoreType.DMA
        ring = dma((3, 2, n // 2 + 1, 2))
        return pl.pallas_call(
            functools.partial(layer_kernel, n, t, heads),
            out_shape=jax.ShapeDtypeStruct((tok, cols), BF16),
            in_specs=[vmem, any_, any_, any_, any_, vmem, vmem, any_, any_, vmem, vmem],
            out_specs=vmem,
            scratch_shapes=[
                pltpu.VMEM((n * tok, 2 * width), BF16),
                pltpu.VMEM((feat, hidden), BF16),
                pltpu.VMEM((feat, hidden), BF16),
                pltpu.VMEM((n, 8, tok), F32),
                pltpu.VMEM((t, width, feat), BF16),
                pltpu.VMEM((t, tok, cols), BF16),
                pltpu.VMEM((heads, tok, 128), F32),
                pltpu.VMEM((tok, width), F32),
                pltpu.VMEM((t, tok, width), BF16),
                pltpu.VMEM((tok, tok), BF16),
                pltpu.VMEM((tok, feat), F32),
                pltpu.VMEM((tok, feat), BF16),
                pltpu.VMEM((tok, hidden), BF16),
                pltpu.VMEM((n, tok, block), BF16),
                pltpu.VMEM((t, per, tok, block), BF16),
                pltpu.VMEM((t, 8, tok), F32),
                ring,
                ring,
                dma((n,)),
                dma((n,)),
                dma((t,)),
                dma((t,)),
                dma((t,)),
                dma((t,)),
                dma((t,)),
                dma((t,)),
                dma((n,)),
                dma((t, per)),
                dma((t,)),
                dma((t,)),
                dma((6,)),
            ],
            compiler_params=pltpu.CompilerParams(
                collective_id=0, has_side_effects=True, vmem_limit_bytes=62 * 1024 * 1024
            ),
        )(
            queries,
            kv,
            br,
            residual_in,
            out_weight,
            first_gain.reshape(1, feat),
            first_shift.reshape(1, feat),
            up_weight,
            down_weight,
            second_gain.reshape(t, 1, cols),
            second_shift.reshape(t, 1, cols),
        )

    return jax.shard_map(
        body,
        mesh=mesh,
        in_specs=(
            P("sp", "tp"),
            P("sp", "tp"),
            P("sp", "tp"),
            P("sp", "tp"),
            P("sp", "tp"),
            P("tp", None),
            P(),
            P(),
            P("sp", "tp"),
            P("sp", "tp"),
            P(),
            P(),
        ),
        out_specs=P("sp", "tp"),
        check_vma=False,
    )
```

profile of v0, /device:TPU:25, one launch (start us, length us, event | category | flops | bytes accessed | tf_op | source)
XLA Modules:
  0.0 221.4 jit_solution(16320019444450343574)
XLA Ops:
  0.0 0.0 copy-start
  0.0 0.7 copy-done
  0.7 0.6 pad_convert_fusion.br_in
  1.3 1.9 pad_maximum_fusion.kv_in
  3.1 216.3 %shard_map.118 = bf16[512,512]{1,0:T(8,128)(2,1)} custom-call(bf16[512,256]{1,0:T(8,128)(2,1)} %q_ref.1, bf16[512,512]{1,0:T(8,128)(2,1)} %pad_maximum_fusion.kv_in, f32[8,512]{1,0:T(8,128)} %pad_convert_fusion.br_in, bf16[512,512]{1,0:T(8,128)(2,1)} %res_in.1, bf16[256,2048]{1,0:T(8,128)(2,1)} %ow_in.1, f32[1,2048]{1,0:T(1,128)} %bitcast.5, ...), custom_call_target="tpu_custom_call" | custom-call | tf_op jit(solution)/shard_map/pallas_call | solution.py:529
  219.5 1.9 copy.14
Async XLA Ops:
  0.0 0.7 copy-start
where the time goes:
time: 225 us; the launch traced here: 221 us
  Pallas kernels  216 us (96%)
  local copies, waits for them, and re-layouts  2.55 us (1%)
  other arithmetic  2.46 us (1%)
    pallas_call x1, Pallas kernels, body(): pl.pallas_call(functools.partial(layer_kernel, n, t, heads), out_shape=ja...  216 us

commit v1 on v0

--- a/solution.py
+++ b/solution.py
@@ -496,6 +496,756 @@
         tp_copy(stat.at[me_t], stat_at, stat_send, stat_recv, d).wait_send()
 
 
+GROUP = 4
+
+
+def flip(a, r):
+    bit = 1
+    out = a
+    while bit <= r:
+        if r & bit:
+            out = out + bit - 2 * bit * lax.rem(a // bit, 2)
+        bit *= 2
+    return out
+
+
+def remote(src, dst, send, recv, **where):
+    return pltpu.make_async_remote_copy(
+        src_ref=src,
+        dst_ref=dst,
+        send_sem=send,
+        recv_sem=recv,
+        device_id=where,
+        device_id_type=MESH,
+    )
+
+
+def grouped_kernel(
+    n,
+    t,
+    q_in,
+    k_in,
+    v_in,
+    br_in,
+    res_in,
+    ow_in,
+    g1_ref,
+    b1_ref,
+    up_in,
+    down_in,
+    g2_ref,
+    b2_ref,
+    out_ref,
+    kvb,
+    qb,
+    br,
+    later_sum,
+    totals,
+    att_own,
+    att_all,
+    tri_ref,
+    ow,
+    res,
+    pre,
+    first,
+    up,
+    down,
+    act,
+    pair_out,
+    pair_in,
+    summed,
+    near_in,
+    cross_out,
+    cross_in,
+    mixed_ref,
+    stat,
+    kv_send,
+    kv_recv,
+    kx_send,
+    kx_recv,
+    br_send,
+    br_recv,
+    ow_send,
+    ow_recv,
+    res_send,
+    res_recv,
+    att_send,
+    att_recv,
+    w_send,
+    w_recv,
+    t1_send,
+    t1_recv,
+    t2_send,
+    t2_recv,
+    t3_send,
+    t3_recv,
+    pair_send,
+    pair_recv,
+    near_send,
+    near_recv,
+    cross_send,
+    cross_recv,
+    stat_send,
+    stat_recv,
+    local_sem,
+    go_sem,
+):
+    s = lax.axis_index("sp")
+    q = lax.axis_index("tp")
+    y = lax.rem(s, 2)
+    z = s // 2
+    levels = n // 2
+    m = lax.rem(s, GROUP)
+    group = s // GROUP
+    x = q // 2
+    c = lax.rem(q, 2)
+    tok, width = q_in.shape
+    hd = width // 2
+    feat = ow.shape[2]
+    cols = feat // t
+    half_feat = feat // 2
+    block = up_in.shape[0]
+    sub = up_in.shape[1] // GROUP
+    part = tok // 2
+    half_n = n // 2
+    sibling = flip(q, 1)
+    across = flip(q, 2)
+
+    barrier = pltpu.get_barrier_semaphore()
+    for r in range(1, n):
+        pl.semaphore_signal(barrier, inc=1, device_id={"sp": flip(s, r)}, device_id_type=MESH)
+    for r in range(1, t):
+        pl.semaphore_signal(barrier, inc=1, device_id={"tp": flip(q, r)}, device_id_type=MESH)
+        pl.semaphore_signal(
+            barrier, inc=1, device_id={"sp": flip(s, 1), "tp": flip(q, r)}, device_id_type=MESH
+        )
+
+    def lanes_of(i, size):
+        return aligned(i * size, size)
+
+    own_copies = [
+        pltpu.make_async_copy(
+            k_in.at[:, lanes_of(y, hd)], kvb.at[s, :, pl.ds(0, hd)], local_sem.at[0]
+        ),
+        pltpu.make_async_copy(
+            v_in.at[:, lanes_of(y, hd)], kvb.at[s, :, pl.ds(hd, hd)], local_sem.at[1]
+        ),
+        pltpu.make_async_copy(q_in.at[:, lanes_of(y, hd)], qb.at[y], local_sem.at[2]),
+    ]
+    other_copies = [
+        pltpu.make_async_copy(br_in, br.at[s], local_sem.at[3]),
+        pltpu.make_async_copy(res_in.at[lanes_of(c, part)], res.at[q], local_sem.at[4]),
+        pltpu.make_async_copy(ow_in, ow.at[q], local_sem.at[5]),
+        pltpu.make_async_copy(
+            up_in.at[:, lanes_of(m, sub)], up.at[lanes_of(s, block)], local_sem.at[6]
+        ),
+        pltpu.make_async_copy(
+            down_in.at[:, lanes_of(m, sub)], down.at[lanes_of(s, block)], local_sem.at[7]
+        ),
+    ]
+    for cp in own_copies:
+        cp.start()
+
+    ps = flip(s, 1)
+    py = 1 - y
+
+    def exchange(landed=False):
+        own = ps if landed else s
+        row = y if landed else py
+        mine = py if landed else y
+        return [
+            remote(
+                kvb.at[own, :, pl.ds(0, hd)] if landed else k_in.at[:, lanes_of(row, hd)],
+                kvb.at[own, :, pl.ds(0, hd)],
+                kx_send.at[0],
+                kx_recv.at[0],
+                sp=ps,
+            ),
+            remote(
+                kvb.at[own, :, pl.ds(hd, hd)] if landed else v_in.at[:, lanes_of(row, hd)],
+                kvb.at[own, :, pl.ds(hd, hd)],
+                kx_send.at[1],
+                kx_recv.at[1],
+                sp=ps,
+            ),
+            remote(
+                qb.at[mine] if landed else q_in.at[:, lanes_of(row, hd)],
+                qb.at[mine],
+                kx_send.at[2],
+                kx_recv.at[2],
+                sp=ps,
+            ),
+        ]
+
+    def relay(slot):
+        return remote(kvb.at[slot], kvb.at[slot], kv_send.at[slot], kv_recv.at[slot], sp=s + 2)
+
+    def relay_landed(slot):
+        return remote(kvb.at[slot], kvb.at[slot], kv_send.at[slot], kv_recv.at[slot], sp=s)
+
+    def br_copy(r, landed=False):
+        owner = flip(s, r) if landed else s
+        return remote(
+            br.at[owner] if landed else br_in,
+            br.at[owner],
+            br_send.at[r],
+            br_recv.at[r],
+            sp=flip(s, r),
+        )
+
+    def ow_copy(r, landed=False):
+        owner = flip(q, r) if landed else q
+        return remote(
+            ow.at[owner] if landed else ow_in,
+            ow.at[owner],
+            ow_send.at[r],
+            ow_recv.at[r],
+            tp=flip(q, r),
+        )
+
+    def res_copy(r, landed=False):
+        to = flip(q, r)
+        owner = to if landed else q
+        return remote(
+            res.at[owner] if landed else res_in.at[lanes_of(lax.rem(to, 2), part)],
+            res.at[owner],
+            res_send.at[r],
+            res_recv.at[r],
+            tp=to,
+        )
+
+    mats_in = (up_in, down_in)
+    mats = (up, down)
+
+    def w_copy(mat, r, landed=False):
+        to = flip(s, r)
+        owner = to if landed else s
+        dst = mats[mat].at[lanes_of(owner, block)]
+        return remote(
+            dst if landed else mats_in[mat].at[:, lanes_of(lax.rem(to, GROUP), sub)],
+            dst,
+            w_send.at[mat, r],
+            w_recv.at[mat, r],
+            sp=to,
+        )
+
+    order = [r for r in range(n - 1, 0, -1)]
+
+    def climbs(r):
+        top = 1
+        while top * 2 <= r:
+            top *= 2
+        if top < 2:
+            return None
+        return lax.rem(s // top, 2) == 0
+
+    def send_mat(mat, upward):
+        for r in order:
+            up_cond = climbs(r)
+
+            def go(r=r):
+                w_copy(mat, r).start()
+
+            if up_cond is None:
+                if not upward:
+                    go()
+            else:
+                pl.when(up_cond if upward else jnp.logical_not(up_cond))(go)
+
+    pl.semaphore_wait(barrier, n - 1 + 2 * (t - 1))
+    for cp in exchange():
+        cp.start()
+    for r in range(1, n):
+        br_copy(r).start()
+    for cp in other_copies:
+        cp.start()
+    for cp in own_copies:
+        cp.wait()
+
+    @pl.when(z < levels - 1)
+    def _():
+        relay(s).start()
+
+    for r in range(1, t):
+        ow_copy(r).start()
+    for r in range(1, t):
+        res_copy(r).start()
+    send_mat(0, False)
+
+    key_row = lax.broadcasted_iota(jnp.int32, tri_ref.shape, 0)
+    key_col = lax.broadcasted_iota(jnp.int32, tri_ref.shape, 1)
+    tri_ref[...] = jnp.where(key_row > key_col, 1.0, 0.0).astype(BF16)
+    later_sum[...] = jnp.zeros_like(later_sum)
+    totals[...] = jnp.zeros_like(totals)
+
+    for cp in exchange(landed=True):
+        cp.wait_recv()
+
+    @pl.when(z < levels - 1)
+    def _():
+        relay(ps).start()
+
+    for r in range(1, n):
+        br_copy(r, landed=True).wait_recv()
+    for cp in other_copies:
+        cp.wait()
+
+    scale = hd ** (-0.5)
+    tile = 128
+    span = tri_ref.shape[0]
+
+    def attend(slot, qy, masked):
+        def rows(i, _):
+            at = aligned(i * tile, tile)
+            z_ = lax.dot_general(
+                qb[qy, at, :],
+                kvb[slot, :, pl.ds(0, hd)],
+                (((1,), (1,)), ((), ())),
+                preferred_element_type=F32,
+            )
+            z_ = z_ * scale + br[slot, pl.ds(y, 1), :]
+            soft = jnp.log(1.0 + jnp.exp(-jnp.abs(z_)))
+            log_break = jnp.minimum(z_, 0.0) - soft
+            keep = log_break - z_
+            if masked:
+                r = lax.broadcasted_iota(jnp.int32, (tile, tok), 0) + i * tile
+                strict = lax.broadcasted_iota(jnp.int32, (tile, tok), 1) < r
+                keep = jnp.where(strict, keep, 0.0)
+            high = keep.astype(BF16)
+            low = (keep - high.astype(F32)).astype(BF16)
+            tri = tri_ref[...]
+            run = later_sum[qy, at, :][:, 0:1]
+            pieces = []
+            for b in range(tok // span - 1, -1, -1):
+                sl = slice(b * span, (b + 1) * span)
+                later = jnp.dot(high[:, sl], tri, preferred_element_type=F32) + jnp.dot(
+                    low[:, sl], tri, preferred_element_type=F32
+                )
+                pieces.append(later + run)
+                run = run + jnp.sum(keep[:, sl], axis=1, keepdims=True)
+            w = jnp.exp(log_break + jnp.concatenate(pieces[::-1], axis=1))
+            if masked:
+                w = jnp.where(strict, w, 0.0)
+            totals[qy, at, :] += jnp.dot(
+                w.astype(BF16), kvb[slot, :, pl.ds(hd, hd)], preferred_element_type=F32
+            )
+            later_sum[qy, at, :] = jnp.broadcast_to(run, (tile, 128))
+            return 0
+
+        lax.fori_loop(0, tok // tile, rows, 0)
+
+    attend(2 * z + 1, 1, True)
+    attend(2 * z, 0, True)
+    attend(2 * z, 1, False)
+
+    def attend_step(k, _):
+        slot = 2 * z + 1 - k
+
+        @pl.when(slot >= 0)
+        def _():
+            relay_landed(slot).wait_recv()
+
+            @pl.when(z < levels - 1)
+            def _():
+                relay(slot).start()
+
+            def one(qy, _):
+                attend(slot, qy, False)
+                return 0
+
+            lax.fori_loop(0, 2, one, 0)
+
+        return 0
+
+    lax.fori_loop(2, n, attend_step, 0)
+
+    @pl.when(z == 1)
+    def _():
+        pl.semaphore_signal(go_sem, inc=1, device_id={"sp": s - 2}, device_id_type=MESH)
+
+    @pl.when(z == 0)
+    def _():
+        pl.semaphore_wait(go_sem, 1)
+
+    send_mat(0, True)
+
+    att_own[...] = totals[...].astype(BF16)
+    att_list = [(dy, r) for dy in range(2) for r in range(t) if dy or r]
+
+    def att_copy(i, landed=False):
+        dy, r = att_list[i]
+        ty = flip(y, 1) if dy else y
+        tq = flip(q, r)
+        sp = ps if dy else s
+        if landed:
+            dst = att_all.at[tq, :, lanes_of(ty, hd)]
+            return remote(dst, dst, att_send.at[i], att_recv.at[i], sp=sp, tp=tq)
+        return remote(
+            att_own.at[ty, lanes_of(lax.rem(tq, 2), part)],
+            att_all.at[q, :, lanes_of(y, hd)],
+            att_send.at[i],
+            att_recv.at[i],
+            sp=sp,
+            tp=tq,
+        )
+
+    for i in range(len(att_list)):
+        att_copy(i).start()
+    att_all[q, :, lanes_of(y, hd)] = att_own[y, lanes_of(c, part), :]
+    for r in range(1, t):
+        ow_copy(r, landed=True).wait_recv()
+        res_copy(r, landed=True).wait_recv()
+    for i in range(len(att_list)):
+        att_copy(i, landed=True).wait_recv()
+
+    for cc in range(t):
+        lanes = pl.ds(cc * cols, cols)
+        mixed = jnp.zeros((part, cols), F32)
+        for g in range(t):
+            mixed = mixed + jnp.dot(
+                att_all[g], ow[g, :, lanes], preferred_element_type=F32
+            ).astype(BF16).astype(F32)
+        pre[:, lanes] = ALPHA * res[cc].astype(F32) + mixed
+
+    small = 64
+
+    def norm_rows(i, _):
+        at = aligned(i * small, small)
+        v = pre[at, :]
+        center = jnp.sum(v, axis=1, keepdims=True) / feat
+        v = v - center
+        spread = jnp.sum(v * v, axis=1, keepdims=True) / feat
+        v = (v * lax.rsqrt(spread + EPSILON) * g1_ref[...] + b1_ref[...]).astype(BF16)
+        first[m, c, 0, at, :] = v[:, :half_feat]
+        first[m, c, 1, at, :] = v[:, half_feat:]
+        return 0
+
+    lax.fori_loop(0, part // small, norm_rows, 0)
+
+    def member(r):
+        return flip(m, r)
+
+    def group_dev(r):
+        return flip(s, r)
+
+    def t1_copy(r, landed=False):
+        ref = first.at[member(r) if landed else m, c, x]
+        return remote(ref, ref, t1_send.at[r], t1_recv.at[r], sp=group_dev(r))
+
+    def t2_copy(r, landed=False):
+        ref = first.at[member(r), c, 1 - x if landed else x]
+        return remote(ref, ref, t2_send.at[r], t2_recv.at[r], tp=across)
+
+    def t3_copy(r, h, landed=False):
+        xh = x if h == 0 else 1 - x
+        ref = first.at[member(r), 1 - c if landed else c, xh]
+        return remote(ref, ref, t3_send.at[r, h], t3_recv.at[r, h], tp=sibling)
+
+    for r in range(GROUP - 1, 0, -1):
+        t1_copy(r).start()
+    for h in range(2):
+        t3_copy(0, h).start()
+    send_mat(1, False)
+    send_mat(1, True)
+
+    steps = (1, 2, 3)
+    for r in range(1, n):
+        w_copy(0, r, landed=True).wait_recv()
+
+    def up_block(mm):
+        def one(i, _):
+            ch = i // 2
+            lanes = aligned(lax.rem(i, 2) * (sub // 2), sub // 2)
+            a = jnp.dot(
+                first[mm, ch, 0], up[pl.ds(0, half_feat), lanes], preferred_element_type=F32
+            ) + jnp.dot(
+                first[mm, ch, 1],
+                up[pl.ds(half_feat, half_feat), lanes],
+                preferred_element_type=F32,
+            )
+            a = jnp.maximum(a, 0.0)
+            act[aligned(mm * tok + ch * part, part), lanes] = (a * a).astype(BF16)
+            return 0
+
+        lax.fori_loop(0, 4, one, 0)
+
+    for h in range(2):
+        t3_copy(0, h, landed=True).wait_recv()
+    for r in steps:
+        t1_copy(r, landed=True).wait_recv()
+        t2_copy(r).start()
+        t3_copy(r, 0).start()
+    up_block(m)
+    for r in steps:
+        t2_copy(r, landed=True).wait_recv()
+        t3_copy(r, 1).start()
+        for h in range(2):
+            t3_copy(r, h, landed=True).wait_recv()
+        up_block(member(r))
+
+    def piece(mm, tq, fh):
+        rows = aligned((tq * (cols // block) + fh) * block, block)
+        return lax.dot_general(
+            act[aligned(mm * tok, tok), :],
+            down[rows, :],
+            (((1,), (1,)), ((), ())),
+            preferred_element_type=F32,
+        )
+
+    def pair_copy(p, mm):
+        return remote(
+            pair_out.at[p, mm],
+            pair_in.at[p, mm],
+            pair_send.at[p, mm],
+            pair_recv.at[p, mm],
+            tp=sibling,
+        )
+
+    def near_copy(p, r, landed=False):
+        return remote(
+            summed.at[p, member(r)],
+            near_in.at[p, r],
+            near_send.at[p, r],
+            near_recv.at[p, r],
+            sp=group_dev(r),
+        )
+
+    def cross_copy():
+        return remote(cross_out, cross_in, cross_send.at[0], cross_recv.at[0], tp=across)
+
+    member_order = (3, 1, 2, 0)
+
+    def reduce_phase(p):
+        xp = group if p == 0 else 1 - group
+        far = range(half_n, n) if p else range(1, half_n)
+        for r in far:
+            w_copy(1, r, landed=True).wait_recv()
+        for r in member_order:
+            mm = member(r)
+            for fh in range(cols // block):
+                pair_out[p, mm, :, pl.ds(fh * block, block)] = piece(
+                    mm, 2 * xp + 1 - c, fh
+                ).astype(BF16)
+            pair_copy(p, mm).start()
+        for r in member_order:
+            mm = member(r)
+            pair_copy(p, mm).wait_recv()
+            for fh in range(cols // block):
+                lanes = pl.ds(fh * block, block)
+                v = piece(mm, 2 * xp + c, fh) + pair_in[p, mm, :, lanes].astype(F32)
+                summed[p, mm, :, lanes] = v.astype(BF16)
+            if r:
+                near_copy(p, r).start()
+
+    def gather_phase(p):
+        xp = group if p == 0 else 1 - group
+        for r in range(1, GROUP):
+            near_copy(p, r).wait_recv()
+
+        def rows(i, _):
+            at = aligned(i * 64, 64)
+            v = summed[p, m, at, :].astype(F32)
+            for r in range(1, GROUP):
+                v = v + near_in[p, r, at, :].astype(F32)
+
+            @pl.when(xp == x)
+            def _():
+                mixed_ref[at, :] = v
+
+            @pl.when(xp != x)
+            def _():
+                cross_out[at, :] = v.astype(BF16)
+
+            return 0
+
+        lax.fori_loop(0, tok // 64, rows, 0)
+
+        @pl.when(xp != x)
+        def _():
+            cross_copy().start()
+
+    reduce_phase(0)
+    reduce_phase(1)
+    gather_phase(0)
+    gather_phase(1)
+    cross_copy().wait_recv()
+
+    row_tile = 128
+    for i in range(tok // row_tile):
+        at = pl.ds(i * row_tile, row_tile)
+        ch = i // (part // row_tile)
+        inner = pl.ds((i % (part // row_tile)) * row_tile, row_tile)
+        v = ALPHA * first[m, ch, x, inner, lanes_of(c, cols)].astype(F32)
+        v = v + (mixed_ref[at, :] + cross_in[at, :].astype(F32))
+        mixed_ref[at, :] = v
+        sums = jnp.sum(v, axis=1, keepdims=True)
+        squares = jnp.sum(v * v, axis=1, keepdims=True)
+        lane = lax.broadcasted_iota(jnp.int32, (row_tile, 128), 1)
+        st = jnp.where(lane == 0, sums, jnp.where(lane == 1, squares, 0.0))
+        stat[q, :, at] = st.T[0:8, :]
+
+    def stat_copy(r, landed=False):
+        owner = flip(q, r) if landed else q
+        return remote(
+            stat.at[owner], stat.at[owner], stat_send.at[r], stat_recv.at[r], tp=flip(q, r)
+        )
+
+    for r in range(1, t):
+        stat_copy(r).start()
+
+    @pl.when(z < levels - 1)
+    def _():
+        def drain(slot, _):
+            relay(slot).wait_send()
+            return 0
+
+        lax.fori_loop(0, 2 * z + 2, drain, 0)
+
+    for cp in exchange():
+        cp.wait_send()
+    for r in range(1, n):
+        br_copy(r).wait_send()
+        w_copy(0, r).wait_send()
+        w_copy(1, r).wait_send()
+    for r in range(1, t):
+        ow_copy(r).wait_send()
+        res_copy(r).wait_send()
+    for i in range(len(att_list)):
+        att_copy(i).wait_send()
+    for r in range(1, GROUP):
+        t1_copy(r).wait_send()
+        t2_copy(r).wait_send()
+        for p in range(2):
+            near_copy(p, r).wait_send()
+    for r in range(GROUP):
+        for h in range(2):
+            t3_copy(r, h).wait_send()
+        for p in range(2):
+            pair_copy(p, r).wait_send()
+    cross_copy().wait_send()
+
+    for r in range(1, t):
+        stat_copy(r, landed=True).wait_recv()
+    for i in range(tok // row_tile):
+        at = pl.ds(i * row_tile, row_tile)
+        st = stat[0, :, at]
+        for g in range(1, t):
+            st = st + stat[g, :, at]
+        st = jnp.concatenate([st, jnp.zeros((120, row_tile), F32)], axis=0).T
+        center = st[:, 0:1] / feat
+        spread = st[:, 1:2] / feat - center * center
+        v = (mixed_ref[at, :] - center) * lax.rsqrt(spread + EPSILON)
+        out_ref[at, :] = (v * g2_ref[q] + b2_ref[q]).astype(BF16)
+    for r in range(1, t):
+        stat_copy(r).wait_send()
+
+
+def grouped_call(n, t, args):
+    (
+        queries,
+        keys,
+        values,
+        breaks,
+        residual_in,
+        out_weight,
+        first_gain,
+        first_shift,
+        up_weight,
+        down_weight,
+        second_gain,
+        second_shift,
+    ) = args
+    tok, width = queries.shape
+    heads = breaks.shape[1]
+    hd = width // heads
+    feat = out_weight.shape[1]
+    cols = residual_in.shape[1]
+    sub = up_weight.shape[1] // GROUP
+    part = tok // 2
+    br = jnp.pad(breaks.astype(F32).T, ((0, 8 - heads), (0, 0)))
+    any_ = pl.BlockSpec(memory_space=pl.ANY)
+    vmem = pl.BlockSpec(memory_space=pltpu.VMEM)
+    dma = pltpu.SemaphoreType.DMA
+    v = pltpu.VMEM
+    return pl.pallas_call(
+        functools.partial(grouped_kernel, n, t),
+        out_shape=jax.ShapeDtypeStruct((tok, cols), BF16),
+        in_specs=[any_] * 6 + [vmem, vmem, any_, any_, vmem, vmem],
+        out_specs=vmem,
+        scratch_shapes=[
+            v((n, tok, 2 * hd), BF16),
+            v((2, tok, hd), BF16),
+            v((n, 8, tok), F32),
+            v((2, tok, 128), F32),
+            v((2, tok, hd), F32),
+            v((2, tok, hd), BF16),
+            v((t, part, width), BF16),
+            v((256, 256), BF16),
+            v((t, width, feat), BF16),
+            v((t, part, cols), BF16),
+            v((part, feat), F32),
+            v((GROUP, 2, 2, part, feat // 2), BF16),
+            v((feat, sub), BF16),
+            v((feat, sub), BF16),
+            v((GROUP * tok, sub), BF16),
+            v((2, GROUP, tok, cols), BF16),
+            v((2, GROUP, tok, cols), BF16),
+            v((2, GROUP, tok, cols), BF16),
+            v((2, GROUP, tok, cols), BF16),
+            v((tok, cols), BF16),
+            v((tok, cols), BF16),
+            v((tok, cols), F32),
+            v((t, 8, tok), F32),
+            dma((n,)),
+            dma((n,)),
+            dma((3,)),
+            dma((3,)),
+            dma((n,)),
+            dma((n,)),
+            dma((t,)),
+            dma((t,)),
+            dma((t,)),
+            dma((t,)),
+            dma((2 * t - 1,)),
+            dma((2 * t - 1,)),
+            dma((2, n)),
+            dma((2, n)),
+            dma((GROUP,)),
+            dma((GROUP,)),
+            dma((GROUP,)),
+            dma((GROUP,)),
+            dma((GROUP, 2)),
+            dma((GROUP, 2)),
+            dma((2, GROUP)),
+            dma((2, GROUP)),
+            dma((2, GROUP)),
+            dma((2, GROUP)),
+            dma((1,)),
+            dma((1,)),
+            dma((t,)),
+            dma((t,)),
+            dma((8,)),
+            pltpu.SemaphoreType.REGULAR,
+        ],
+        compiler_params=pltpu.CompilerParams(
+            collective_id=0, has_side_effects=True, vmem_limit_bytes=62 * 1024 * 1024
+        ),
+    )(
+        queries,
+        keys,
+        values,
+        br,
+        residual_in,
+        out_weight,
+        first_gain.reshape(1, feat),
+        first_shift.reshape(1, feat),
+        up_weight,
+        down_weight,
+        second_gain.reshape(t, 1, cols),
+        second_shift.reshape(t, 1, cols),
+    )
+
+
 def solution(mesh):
     n, t = mesh.shape["sp"], mesh.shape["tp"]
 
@@ -515,6 +1265,25 @@
     ):
         tok, width = queries.shape
         heads = breaks.shape[1]
+        if heads == 2 and t == 4 and n == 2 * GROUP:
+            return grouped_call(
+                n,
+                t,
+                (
+                    queries,
+                    keys,
+                    values,
+                    breaks,
+                    residual_in,
+                    out_weight,
+                    first_gain,
+                    first_shift,
+                    up_weight,
+                    down_weight,
+                    second_gain,
+                    second_shift,
+                ),
+            )
         feat = out_weight.shape[1]
         cols = residual_in.shape[1]
         hidden = up_weight.shape[1]

time: 225 us -> 238 us (1.058)
  Pallas kernels: 216 us -> 231 us
    pallas_call x1, Pallas kernels: 216 us -> 231 us  [grouped_call(): pl.pallas_call(functools.partial(grouped_kernel, n, t), out_shape=jax.Sha...]
where the time goes in v1:
time: 238 us; the launch traced here: 234 us
  Pallas kernels  231 us (97%)
  local copies, waits for them, and re-layouts  2.55 us (1%)
    pallas_call x1, Pallas kernels, grouped_call(): pl.pallas_call(functools.partial(grouped_kernel, n, t), out_shape=jax.Sha...  231 us

profile of v1, /device:TPU:25, one launch (start us, length us, event | category | flops | bytes accessed | tf_op | source)
XLA Modules:
  0.0 233.7 jit_solution(18302355962708517595)
XLA Ops:
  0.0 0.0 copy-start
  0.0 0.7 copy-done
  0.7 0.6 pad_convert_fusion.br_in
  1.3 230.5 %shard_map.118 = bf16[512,512]{1,0:T(8,128)(2,1)} custom-call(bf16[512,256]{1,0:T(8,128)(2,1)} %q_in.1, bf16[512,256]{1,0:T(8,128)(2,1)} %k_in.1, bf16[512,256]{1,0:T(8,128)(2,1)} %v_in.1, f32[8,512]{1,0:T(8,128)} %pad_convert_fusion.br_in, bf16[512,512]{1,0:T(8,128)(2,1)} %res_in.1, bf16[256,2048]{1,0:T(8,128)(2,1)} %ow_in.1, f32[1,2048]{1,0:T(1,128)} %bitcast.5, ...), custom_call_target="tpu_custom_call" | custom-call | tf_op jit(solution)/shard_map/pallas_call | solution.py:1170
  231.8 1.9 copy.14
Async XLA Ops:
  0.0 0.7 copy-start

commit v2 on v1

--- a/solution.py
+++ b/solution.py
@@ -555,6 +555,9 @@
     pair_in,
     summed,
     near_in,
+    held,
+    side_out,
+    side_in,
     cross_out,
     cross_in,
     mixed_ref,
@@ -583,6 +586,8 @@
     pair_recv,
     near_send,
     near_recv,
+    side_send,
+    side_recv,
     cross_send,
     cross_recv,
     stat_send,
@@ -689,7 +694,7 @@
             br.at[owner] if landed else br_in,
             br.at[owner],
             br_send.at[r],
-            br_recv.at[r],
+            br_recv.at[owner],
             sp=flip(s, r),
         )
 
@@ -702,6 +707,10 @@
             ow_recv.at[r],
             tp=flip(q, r),
         )
+
+    def ow_pass(landed=False):
+        ref = ow.at[flip(q, 3) if landed else across]
+        return remote(ref, ref, ow_send.at[3], ow_recv.at[3], tp=sibling)
 
     def res_copy(r, landed=False):
         to = flip(q, r)
@@ -729,28 +738,40 @@
             sp=to,
         )
 
-    order = [r for r in range(n - 1, 0, -1)]
-
     def climbs(r):
-        top = 1
-        while top * 2 <= r:
-            top *= 2
-        if top < 2:
-            return None
-        return lax.rem(s // top, 2) == 0
-
-    def send_mat(mat, upward):
-        for r in order:
-            up_cond = climbs(r)
+        return lax.rem(s // (half_n if r >= half_n else 2), 2) == 0
+
+    def send_mat(mat, rs, upward):
+        for r in rs:
 
             def go(r=r):
                 w_copy(mat, r).start()
 
-            if up_cond is None:
-                if not upward:
-                    go()
+            if r < 2:
+                go()
             else:
-                pl.when(up_cond if upward else jnp.logical_not(up_cond))(go)
+                pl.when(climbs(r) if upward else jnp.logical_not(climbs(r)))(go)
+
+    def send_up(mat, skip=()):
+        far_level = [r for r in range(half_n, n) if (r // 2) % 2 and r not in skip]
+        same_level = [r for r in range(half_n, n) if not (r // 2) % 2 and r not in skip]
+
+        @pl.when(group == 0)
+        def _():
+            @pl.when(lax.rem(z, 2) == 0)
+            def _():
+                for r in same_level + far_level:
+                    w_copy(mat, r).start()
+
+            @pl.when(lax.rem(z, 2) == 1)
+            def _():
+                for r in far_level + same_level:
+                    w_copy(mat, r).start()
+
+        send_mat(mat, (2, 3), True)
+
+    straight = [r for r in range(n - 1, 0, -1) if r % 2 == 0]
+    turning = [r for r in range(n - 1, 0, -1) if r % 2]
 
     pl.semaphore_wait(barrier, n - 1 + 2 * (t - 1))
     for cp in exchange():
@@ -767,10 +788,17 @@
         relay(s).start()
 
     for r in range(1, t):
+        res_copy(r).start()
+    for r in (1, 2):
         ow_copy(r).start()
-    for r in range(1, t):
-        res_copy(r).start()
-    send_mat(0, False)
+    send_mat(0, straight, False)
+
+    inner = lax.rem(z, 2) != group
+    far_straight = [r for r in straight if r >= half_n]
+
+    @pl.when(inner)
+    def _():
+        send_mat(1, far_straight, False)
 
     key_row = lax.broadcasted_iota(jnp.int32, tri_ref.shape, 0)
     key_col = lax.broadcasted_iota(jnp.int32, tri_ref.shape, 1)
@@ -778,17 +806,11 @@
     later_sum[...] = jnp.zeros_like(later_sum)
     totals[...] = jnp.zeros_like(totals)
 
-    for cp in exchange(landed=True):
-        cp.wait_recv()
-
-    @pl.when(z < levels - 1)
-    def _():
-        relay(ps).start()
-
-    for r in range(1, n):
-        br_copy(r, landed=True).wait_recv()
     for cp in other_copies:
         cp.wait()
+
+    def br_landed(slot):
+        remote(br.at[slot], br.at[slot], br_send.at[0], br_recv.at[slot], sp=s).wait_recv()
 
     scale = hd ** (-0.5)
     tile = 128
@@ -834,21 +856,46 @@
 
         lax.fori_loop(0, tok // tile, rows, 0)
 
-    attend(2 * z + 1, 1, True)
-    attend(2 * z, 0, True)
-    attend(2 * z, 1, False)
-
-    def attend_step(k, _):
-        slot = 2 * z + 1 - k
-
+    attend(s, y, True)
+    for cp in exchange(landed=True):
+        cp.wait_recv()
+
+    @pl.when(z < levels - 1)
+    def _():
+        relay(ps).start()
+
+    br_landed(ps)
+    send_mat(0, turning, False)
+    attend(ps, py, True)
+
+    def fetch(slot):
         @pl.when(slot >= 0)
         def _():
             relay_landed(slot).wait_recv()
+            br_landed(slot)
 
             @pl.when(z < levels - 1)
             def _():
                 relay(slot).start()
 
+    ahead = jnp.where(z < levels - 1, 2, 0)
+
+    @pl.when(z < levels - 1)
+    def _():
+        fetch(2 * z - 1)
+
+    attend(2 * z, 1, False)
+
+    @pl.when(z < levels - 1)
+    def _():
+        fetch(2 * z - 2)
+
+    def attend_step(k, _):
+        slot = 2 * z + 1 - k
+        fetch(slot - ahead)
+
+        @pl.when(slot >= 0)
+        def _():
             def one(qy, _):
                 attend(slot, qy, False)
                 return 0
@@ -859,6 +906,14 @@
 
     lax.fori_loop(2, n, attend_step, 0)
 
+    @pl.when(z < levels - 1)
+    def _():
+        def drain(slot, _):
+            relay(slot).wait_send()
+            return 0
+
+        lax.fori_loop(0, 2 * z + 2, drain, 0)
+
     @pl.when(z == 1)
     def _():
         pl.semaphore_signal(go_sem, inc=1, device_id={"sp": s - 2}, device_id_type=MESH)
@@ -867,7 +922,14 @@
     def _():
         pl.semaphore_wait(go_sem, 1)
 
-    send_mat(0, True)
+    send_up(0)
+
+    @pl.when(inner)
+    def _():
+        send_mat(1, far_straight, True)
+
+    ow_copy(2, landed=True).wait_recv()
+    ow_pass().start()
 
     att_own[...] = totals[...].astype(BF16)
     att_list = [(dy, r) for dy in range(2) for r in range(t) if dy or r]
@@ -892,8 +954,9 @@
     for i in range(len(att_list)):
         att_copy(i).start()
     att_all[q, :, lanes_of(y, hd)] = att_own[y, lanes_of(c, part), :]
+    ow_copy(1, landed=True).wait_recv()
+    ow_pass(landed=True).wait_recv()
     for r in range(1, t):
-        ow_copy(r, landed=True).wait_recv()
         res_copy(r, landed=True).wait_recv()
     for i in range(len(att_list)):
         att_copy(i, landed=True).wait_recv()
@@ -928,29 +991,38 @@
     def group_dev(r):
         return flip(s, r)
 
-    def t1_copy(r, landed=False):
-        ref = first.at[member(r) if landed else m, c, x]
-        return remote(ref, ref, t1_send.at[r], t1_recv.at[r], sp=group_dev(r))
-
-    def t2_copy(r, landed=False):
-        ref = first.at[member(r), c, 1 - x if landed else x]
-        return remote(ref, ref, t2_send.at[r], t2_recv.at[r], tp=across)
-
-    def t3_copy(r, h, landed=False):
+    quarter = part // 2
+
+    def t1_copy(r, e, landed=False):
+        owner = member(r) if landed else (member(2) if r == 3 else m)
+        ref = first.at[owner, c, x, pl.ds(e * quarter, quarter)]
+        return remote(
+            ref, ref, t1_send.at[r, e], t1_recv.at[r, e], sp=group_dev(1 if r == 3 else r)
+        )
+
+    def t2_copy(r, e, landed=False):
+        ref = first.at[member(r), c, 1 - x if landed else x, pl.ds(e * quarter, quarter)]
+        return remote(ref, ref, t2_send.at[r, e], t2_recv.at[r, e], tp=across)
+
+    def t3_copy(r, h, e, landed=False):
         xh = x if h == 0 else 1 - x
-        ref = first.at[member(r), 1 - c if landed else c, xh]
-        return remote(ref, ref, t3_send.at[r, h], t3_recv.at[r, h], tp=sibling)
-
-    for r in range(GROUP - 1, 0, -1):
-        t1_copy(r).start()
-    for h in range(2):
-        t3_copy(0, h).start()
-    send_mat(1, False)
-    send_mat(1, True)
-
-    steps = (1, 2, 3)
-    for r in range(1, n):
-        w_copy(0, r, landed=True).wait_recv()
+        ref = first.at[member(r), 1 - c if landed else c, xh, pl.ds(e * quarter, quarter)]
+        return remote(ref, ref, t3_send.at[r, h, e], t3_recv.at[r, h, e], tp=sibling)
+
+    for e in range(2):
+        for r in (2, 1):
+            t1_copy(r, e).start()
+    for e in range(2):
+        for h in range(2):
+            t3_copy(0, h, e).start()
+    send_mat(1, [r for r in straight if r < half_n] + turning, False)
+
+    @pl.when(jnp.logical_not(inner))
+    def _():
+        send_mat(1, far_straight, False)
+        send_mat(1, far_straight, True)
+
+    send_up(1, far_straight)
 
     def up_block(mm):
         def one(i, _):
@@ -969,18 +1041,25 @@
 
         lax.fori_loop(0, 4, one, 0)
 
-    for h in range(2):
-        t3_copy(0, h, landed=True).wait_recv()
-    for r in steps:
-        t1_copy(r, landed=True).wait_recv()
-        t2_copy(r).start()
-        t3_copy(r, 0).start()
+    for r, e in ((2, 0), (1, 0), (2, 1), (1, 1), (3, 0), (3, 1)):
+        t1_copy(r, e, landed=True).wait_recv()
+        if r == 2:
+            t1_copy(3, e).start()
+        t2_copy(r, e).start()
+        t3_copy(r, 0, e).start()
+    for e in range(2):
+        for h in range(2):
+            t3_copy(0, h, e, landed=True).wait_recv()
+    for r in range(1, n):
+        w_copy(0, r, landed=True).wait_recv()
     up_block(m)
-    for r in steps:
-        t2_copy(r, landed=True).wait_recv()
-        t3_copy(r, 1).start()
-        for h in range(2):
-            t3_copy(r, h, landed=True).wait_recv()
+    for r in (2, 1, 3):
+        for e in range(2):
+            t2_copy(r, e, landed=True).wait_recv()
+            t3_copy(r, 1, e).start()
+        for e in range(2):
+            for h in range(2):
+                t3_copy(r, h, e, landed=True).wait_recv()
         up_block(member(r))
 
     def piece(mm, tq, fh):
@@ -1001,14 +1080,17 @@
             tp=sibling,
         )
 
-    def near_copy(p, r, landed=False):
+    def near_copy(p, h, r):
         return remote(
-            summed.at[p, member(r)],
-            near_in.at[p, r],
-            near_send.at[p, r],
-            near_recv.at[p, r],
+            summed.at[p, h, member(r)],
+            near_in.at[p, h, r],
+            near_send.at[p, h, r],
+            near_recv.at[p, h, r],
             sp=group_dev(r),
         )
+
+    def side_copy(mm):
+        return remote(side_out.at[mm], side_in.at[mm], side_send.at[mm], side_recv.at[mm], tp=across)
 
     def cross_copy():
         return remote(cross_out, cross_in, cross_send.at[0], cross_recv.at[0], tp=across)
@@ -1022,7 +1104,7 @@
             w_copy(1, r, landed=True).wait_recv()
         for r in member_order:
             mm = member(r)
-            for fh in range(cols // block):
+            for fh in range(2):
                 pair_out[p, mm, :, pl.ds(fh * block, block)] = piece(
                     mm, 2 * xp + 1 - c, fh
                 ).astype(BF16)
@@ -1030,44 +1112,73 @@
         for r in member_order:
             mm = member(r)
             pair_copy(p, mm).wait_recv()
-            for fh in range(cols // block):
-                lanes = pl.ds(fh * block, block)
-                v = piece(mm, 2 * xp + c, fh) + pair_in[p, mm, :, lanes].astype(F32)
-                summed[p, mm, :, lanes] = v.astype(BF16)
+            v = piece(mm, 2 * xp + c, 1) + pair_in[p, mm, :, pl.ds(block, block)].astype(F32)
+            summed[p, 1, mm] = v.astype(BF16)
             if r:
-                near_copy(p, r).start()
-
-    def gather_phase(p):
-        xp = group if p == 0 else 1 - group
-        for r in range(1, GROUP):
-            near_copy(p, r).wait_recv()
-
-        def rows(i, _):
-            at = aligned(i * 64, 64)
-            v = summed[p, m, at, :].astype(F32)
-            for r in range(1, GROUP):
-                v = v + near_in[p, r, at, :].astype(F32)
+                near_copy(p, 1, r).start()
+            v = piece(mm, 2 * xp + c, 0) + pair_in[p, mm, :, pl.ds(0, block)].astype(F32)
 
             @pl.when(xp == x)
             def _():
-                mixed_ref[at, :] = v
+                held[mm] = v
 
             @pl.when(xp != x)
             def _():
-                cross_out[at, :] = v.astype(BF16)
-
-            return 0
-
-        lax.fori_loop(0, tok // 64, rows, 0)
-
-        @pl.when(xp != x)
+                side_out[mm] = v.astype(BF16)
+                side_copy(mm).start()
+
+    def side_phase(p):
+        xp = group if p == 0 else 1 - group
+
+        @pl.when(xp == x)
         def _():
-            cross_copy().start()
+            for r in member_order:
+                mm = member(r)
+                side_copy(mm).wait_recv()
+                if r:
+                    summed[p, 0, mm] = (held[mm] + side_in[mm].astype(F32)).astype(BF16)
+                    near_copy(p, 0, r).start()
+
+    def gather_phase(p, mine):
+        xp = group if p == 0 else 1 - group
+
+        def total(at):
+            v = summed[p, 1, m, at, :].astype(F32)
+            for r in range(1, GROUP):
+                v = v + near_in[p, 1, r, at, :].astype(F32)
+            return v
+
+        @pl.when(xp == x if mine else xp != x)
+        def _():
+            for r in range(1, GROUP):
+                near_copy(p, 1, r).wait_recv()
+                if mine:
+                    near_copy(p, 0, r).wait_recv()
+
+            def rows(i, _):
+                at = aligned(i * 64, 64)
+                if mine:
+                    mixed_ref[at, pl.ds(block, block)] = total(at)
+                    v = held[m, at, :] + side_in[m, at, :].astype(F32)
+                    for r in range(1, GROUP):
+                        v = v + near_in[p, 0, r, at, :].astype(F32)
+                    mixed_ref[at, pl.ds(0, block)] = v
+                else:
+                    cross_out[at, :] = total(at).astype(BF16)
+                return 0
+
+            lax.fori_loop(0, tok // 64, rows, 0)
+            if not mine:
+                cross_copy().start()
 
     reduce_phase(0)
     reduce_phase(1)
-    gather_phase(0)
-    gather_phase(1)
+    side_phase(0)
+    side_phase(1)
+    for p in range(2):
+        gather_phase(p, False)
+    for p in range(2):
+        gather_phase(p, True)
     cross_copy().wait_recv()
 
     row_tile = 128
@@ -1076,7 +1187,13 @@
         ch = i // (part // row_tile)
         inner = pl.ds((i % (part // row_tile)) * row_tile, row_tile)
         v = ALPHA * first[m, ch, x, inner, lanes_of(c, cols)].astype(F32)
-        v = v + (mixed_ref[at, :] + cross_in[at, :].astype(F32))
+        v = v + jnp.concatenate(
+            [
+                mixed_ref[at, pl.ds(0, block)],
+                mixed_ref[at, pl.ds(block, block)] + cross_in[at, :].astype(F32),
+            ],
+            axis=1,
+        )
         mixed_ref[at, :] = v
         sums = jnp.sum(v, axis=1, keepdims=True)
         squares = jnp.sum(v * v, axis=1, keepdims=True)
@@ -1093,35 +1210,38 @@
     for r in range(1, t):
         stat_copy(r).start()
 
-    @pl.when(z < levels - 1)
-    def _():
-        def drain(slot, _):
-            relay(slot).wait_send()
-            return 0
-
-        lax.fori_loop(0, 2 * z + 2, drain, 0)
-
     for cp in exchange():
         cp.wait_send()
+    def br_rest(slot, _):
+        br_landed(slot)
+        return 0
+
+    lax.fori_loop(2 * z + 2, n, br_rest, 0)
     for r in range(1, n):
         br_copy(r).wait_send()
         w_copy(0, r).wait_send()
         w_copy(1, r).wait_send()
+    for r in (1, 2):
+        ow_copy(r).wait_send()
+    ow_pass().wait_send()
     for r in range(1, t):
-        ow_copy(r).wait_send()
         res_copy(r).wait_send()
     for i in range(len(att_list)):
         att_copy(i).wait_send()
     for r in range(1, GROUP):
-        t1_copy(r).wait_send()
-        t2_copy(r).wait_send()
+        for e in range(2):
+            t1_copy(r, e).wait_send()
+            t2_copy(r, e).wait_send()
         for p in range(2):
-            near_copy(p, r).wait_send()
+            near_copy(p, 1, r).wait_send()
+        near_copy(jnp.where(group == x, 0, 1), 0, r).wait_send()
     for r in range(GROUP):
         for h in range(2):
-            t3_copy(r, h).wait_send()
+            for e in range(2):
+                t3_copy(r, h, e).wait_send()
         for p in range(2):
             pair_copy(p, r).wait_send()
+        side_copy(r).wait_send()
     cross_copy().wait_send()
 
     for r in range(1, t):
@@ -1190,10 +1310,13 @@
             v((GROUP * tok, sub), BF16),
             v((2, GROUP, tok, cols), BF16),
             v((2, GROUP, tok, cols), BF16),
-            v((2, GROUP, tok, cols), BF16),
-            v((2, GROUP, tok, cols), BF16),
-            v((tok, cols), BF16),
-            v((tok, cols), BF16),
+            v((2, 2, GROUP, tok, cols // 2), BF16),
+            v((2, 2, GROUP, tok, cols // 2), BF16),
+            v((GROUP, tok, cols // 2), F32),
+            v((GROUP, tok, cols // 2), BF16),
+            v((GROUP, tok, cols // 2), BF16),
+            v((tok, cols // 2), BF16),
+            v((tok, cols // 2), BF16),
             v((tok, cols), F32),
             v((t, 8, tok), F32),
             dma((n,)),
@@ -1210,16 +1333,18 @@
             dma((2 * t - 1,)),
             dma((2, n)),
             dma((2, n)),
+            dma((GROUP, 2)),
+            dma((GROUP, 2)),
+            dma((GROUP, 2)),
+            dma((GROUP, 2)),
+            dma((GROUP, 2, 2)),
+            dma((GROUP, 2, 2)),
+            dma((2, GROUP)),
+            dma((2, GROUP)),
+            dma((2, 2, GROUP)),
+            dma((2, 2, GROUP)),
             dma((GROUP,)),
             dma((GROUP,)),
-            dma((GROUP,)),
-            dma((GROUP,)),
-            dma((GROUP, 2)),
-            dma((GROUP, 2)),
-            dma((2, GROUP)),
-            dma((2, GROUP)),
-            dma((2, GROUP)),
-            dma((2, GROUP)),
             dma((1,)),
             dma((1,)),
             dma((t,)),

time: 238 us -> 180 us (0.76); the launches traced: 234 us -> 180 us
  Pallas kernels: 231 us -> 177 us
    pallas_call x1, Pallas kernels: 231 us -> 177 us  [grouped_call(): pl.pallas_call(functools.partial(grouped_kernel, n, t), out_shape=jax.Sha...]
where the time goes in v2:
time: 180 us
  Pallas kernels  177 us (98%)
  local copies, waits for them, and re-layouts  2.55 us (1%)
    pallas_call x1, Pallas kernels, grouped_call(): pl.pallas_call(functools.partial(grouped_kernel, n, t), out_shape=jax.Sha...  177 us

profile of v2, /device:TPU:25, one launch (start us, length us, event | category | flops | bytes accessed | tf_op | source)
XLA Modules:
  0.0 180.0 jit_solution(5223072279254463935)
XLA Ops:
  0.0 0.0 copy-start
  0.0 0.7 copy-done
  0.7 0.6 pad_convert_fusion.br_in
  1.3 176.9 %shard_map.118 = bf16[512,512]{1,0:T(8,128)(2,1)} custom-call(bf16[512,256]{1,0:T(8,128)(2,1)} %q_in.1, bf16[512,256]{1,0:T(8,128)(2,1)} %k_in.1, bf16[512,256]{1,0:T(8,128)(2,1)} %v_in.1, f32[8,512]{1,0:T(8,128)} %pad_convert_fusion.br_in, bf16[512,512]{1,0:T(8,128)(2,1)} %res_in.1, bf16[256,2048]{1,0:T(8,128)(2,1)} %ow_in.1, f32[1,2048]{1,0:T(1,128)} %bitcast.5, ...), custom_call_target="tpu_custom_call" | custom-call | tf_op jit(solution)/shard_map/pallas_call | solution.py:1290
  178.2 1.9 %copy.14 = bf16[512,512]{1,0:T(8,128)(2,1)} copy(bf16[512,512]{1,0:T(8,128)(2,1)} %shard_map.118) | data formatting | bytes 1048576
Async XLA Ops:
  0.0 0.7 copy-start

commit v3 on v2

--- a/solution.py
+++ b/solution.py
@@ -594,6 +594,7 @@
     stat_recv,
     local_sem,
     go_sem,
+    pair_sem,
 ):
     s = lax.axis_index("sp")
     q = lax.axis_index("tp")
@@ -768,8 +769,6 @@
                 for r in far_level + same_level:
                     w_copy(mat, r).start()
 
-        send_mat(mat, (2, 3), True)
-
     straight = [r for r in range(n - 1, 0, -1) if r % 2 == 0]
     turning = [r for r in range(n - 1, 0, -1) if r % 2]
 
@@ -796,10 +795,6 @@
     inner = lax.rem(z, 2) != group
     far_straight = [r for r in straight if r >= half_n]
 
-    @pl.when(inner)
-    def _():
-        send_mat(1, far_straight, False)
-
     key_row = lax.broadcasted_iota(jnp.int32, tri_ref.shape, 0)
     key_col = lax.broadcasted_iota(jnp.int32, tri_ref.shape, 1)
     tri_ref[...] = jnp.where(key_row > key_col, 1.0, 0.0).astype(BF16)
@@ -813,7 +808,7 @@
         remote(br.at[slot], br.at[slot], br_send.at[0], br_recv.at[slot], sp=s).wait_recv()
 
     scale = hd ** (-0.5)
-    tile = 128
+    tile = 512
     span = tri_ref.shape[0]
 
     def attend(slot, qy, masked):
@@ -913,6 +908,10 @@
             return 0
 
         lax.fori_loop(0, 2 * z + 2, drain, 0)
+        pl.semaphore_signal(pair_sem, inc=1, device_id={"tp": sibling}, device_id_type=MESH)
+        pl.semaphore_wait(pair_sem, 1)
+
+    send_mat(0, (2, 3), True)
 
     @pl.when(z == 1)
     def _():
@@ -926,6 +925,7 @@
 
     @pl.when(inner)
     def _():
+        send_mat(1, far_straight, False)
         send_mat(1, far_straight, True)
 
     ow_copy(2, landed=True).wait_recv()
@@ -1015,14 +1015,14 @@
     for e in range(2):
         for h in range(2):
             t3_copy(0, h, e).start()
-    send_mat(1, [r for r in straight if r < half_n] + turning, False)
+    send_mat(1, [r for r in straight if r < half_n], False)
 
     @pl.when(jnp.logical_not(inner))
     def _():
         send_mat(1, far_straight, False)
         send_mat(1, far_straight, True)
 
-    send_up(1, far_straight)
+    send_mat(1, (2,), True)
 
     def up_block(mm):
         def one(i, _):
@@ -1041,19 +1041,27 @@
 
         lax.fori_loop(0, 4, one, 0)
 
-    for r, e in ((2, 0), (1, 0), (2, 1), (1, 1), (3, 0), (3, 1)):
-        t1_copy(r, e, landed=True).wait_recv()
-        if r == 2:
-            t1_copy(3, e).start()
-        t2_copy(r, e).start()
-        t3_copy(r, 0, e).start()
+    def pass_on(steps):
+        for r, e in steps:
+            t1_copy(r, e, landed=True).wait_recv()
+            if r == 2:
+                t1_copy(3, e).start()
+            t2_copy(r, e).start()
+            t3_copy(r, 0, e).start()
+
+    pass_on(((1, 0), (2, 0), (1, 1), (2, 1)))
+    send_mat(1, [r for r in turning if r > 1], False)
+    send_mat(1, (1,), False)
+    send_mat(1, (3,), True)
+    send_up(1, far_straight)
     for e in range(2):
         for h in range(2):
             t3_copy(0, h, e, landed=True).wait_recv()
     for r in range(1, n):
         w_copy(0, r, landed=True).wait_recv()
     up_block(m)
-    for r in (2, 1, 3):
+    pass_on(((3, 0), (3, 1)))
+    for r in (1, 2, 3):
         for e in range(2):
             t2_copy(r, e, landed=True).wait_recv()
             t3_copy(r, 1, e).start()
@@ -1086,8 +1094,14 @@
             near_in.at[p, h, r],
             near_send.at[p, h, r],
             near_recv.at[p, h, r],
-            sp=group_dev(r),
-        )
+            sp=group_dev(2 if r == 2 else 1),
+        )
+
+    def near_on(p, h):
+        near_copy(p, h, 3).wait_recv()
+        both = summed[p, h, member(2)].astype(F32) + near_in[p, h, 3].astype(F32)
+        summed[p, h, member(2)] = both.astype(BF16)
+        near_copy(p, h, 2).start()
 
     def side_copy(mm):
         return remote(side_out.at[mm], side_in.at[mm], side_send.at[mm], side_recv.at[mm], tp=across)
@@ -1114,43 +1128,46 @@
             pair_copy(p, mm).wait_recv()
             v = piece(mm, 2 * xp + c, 1) + pair_in[p, mm, :, pl.ds(block, block)].astype(F32)
             summed[p, 1, mm] = v.astype(BF16)
-            if r:
+            if r % 2:
                 near_copy(p, 1, r).start()
             v = piece(mm, 2 * xp + c, 0) + pair_in[p, mm, :, pl.ds(0, block)].astype(F32)
 
             @pl.when(xp == x)
             def _():
-                held[mm] = v
+                held[p, mm] = v
 
             @pl.when(xp != x)
             def _():
                 side_out[mm] = v.astype(BF16)
                 side_copy(mm).start()
 
-    def side_phase(p):
+    def side_phase(p, rs):
         xp = group if p == 0 else 1 - group
 
         @pl.when(xp == x)
         def _():
-            for r in member_order:
+            for r in rs:
                 mm = member(r)
                 side_copy(mm).wait_recv()
                 if r:
-                    summed[p, 0, mm] = (held[mm] + side_in[mm].astype(F32)).astype(BF16)
+                    summed[p, 0, mm] = (held[p, mm] + side_in[mm].astype(F32)).astype(BF16)
+                if r % 2:
                     near_copy(p, 0, r).start()
+            if 0 in rs:
+                near_on(p, 0)
 
     def gather_phase(p, mine):
         xp = group if p == 0 else 1 - group
 
         def total(at):
             v = summed[p, 1, m, at, :].astype(F32)
-            for r in range(1, GROUP):
+            for r in (1, 2):
                 v = v + near_in[p, 1, r, at, :].astype(F32)
             return v
 
         @pl.when(xp == x if mine else xp != x)
         def _():
-            for r in range(1, GROUP):
+            for r in (1, 2):
                 near_copy(p, 1, r).wait_recv()
                 if mine:
                     near_copy(p, 0, r).wait_recv()
@@ -1159,8 +1176,8 @@
                 at = aligned(i * 64, 64)
                 if mine:
                     mixed_ref[at, pl.ds(block, block)] = total(at)
-                    v = held[m, at, :] + side_in[m, at, :].astype(F32)
-                    for r in range(1, GROUP):
+                    v = held[p, m, at, :] + side_in[m, at, :].astype(F32)
+                    for r in (1, 2):
                         v = v + near_in[p, 0, r, at, :].astype(F32)
                     mixed_ref[at, pl.ds(0, block)] = v
                 else:
@@ -1173,10 +1190,14 @@
 
     reduce_phase(0)
     reduce_phase(1)
-    side_phase(0)
-    side_phase(1)
+    near_on(0, 1)
     for p in range(2):
-        gather_phase(p, False)
+        side_phase(p, member_order[:2])
+    gather_phase(0, False)
+    near_on(1, 1)
+    for p in range(2):
+        side_phase(p, member_order[2:])
+    gather_phase(1, False)
     for p in range(2):
         gather_phase(p, True)
     cross_copy().wait_recv()
@@ -1312,7 +1333,7 @@
             v((2, GROUP, tok, cols), BF16),
             v((2, 2, GROUP, tok, cols // 2), BF16),
             v((2, 2, GROUP, tok, cols // 2), BF16),
-            v((GROUP, tok, cols // 2), F32),
+            v((2, GROUP, tok, cols // 2), F32),
             v((GROUP, tok, cols // 2), BF16),
             v((GROUP, tok, cols // 2), BF16),
             v((tok, cols // 2), BF16),
@@ -1350,6 +1371,7 @@
             dma((t,)),
             dma((t,)),
             dma((8,)),
+            pltpu.SemaphoreType.REGULAR,
             pltpu.SemaphoreType.REGULAR,
         ],
         compiler_params=pltpu.CompilerParams(

time: 180 us -> 173 us (0.961); the launches traced: 180 us -> 170 us
  Pallas kernels: 177 us -> 167 us
    pallas_call x1, Pallas kernels: 177 us -> 167 us  [grouped_call(): pl.pallas_call(functools.partial(grouped_kernel, n, t), out_shape=jax.Sha...]
where the time goes in v3:
time: 173 us; the launch traced here: 170 us
  Pallas kernels  167 us (97%)
  local copies, waits for them, and re-layouts  2.55 us (1%)
    pallas_call x1, Pallas kernels, grouped_call(): pl.pallas_call(functools.partial(grouped_kernel, n, t), out_shape=jax.Sha...  167 us

profile of v3, /device:TPU:25, one launch (start us, length us, event | category | flops | bytes accessed | tf_op | source)
XLA Modules:
  0.0 170.4 jit_solution(8069997150198096115)
XLA Ops:
  0.0 0.0 copy-start
  0.0 0.7 copy-done
  0.7 0.6 pad_convert_fusion.br_in
  1.3 167.3 %shard_map.118 = bf16[512,512]{1,0:T(8,128)(2,1)} custom-call(bf16[512,256]{1,0:T(8,128)(2,1)} %q_in.1, bf16[512,256]{1,0:T(8,128)(2,1)} %k_in.1, bf16[512,256]{1,0:T(8,128)(2,1)} %v_in.1, f32[8,512]{1,0:T(8,128)} %pad_convert_fusion.br_in, bf16[512,512]{1,0:T(8,128)(2,1)} %res_in.1, bf16[256,2048]{1,0:T(8,128)(2,1)} %ow_in.1, f32[1,2048]{1,0:T(1,128)} %bitcast.5, ...), custom_call_target="tpu_custom_call" | custom-call | tf_op jit(solution)/shard_map/pallas_call | solution.py:1311
  168.6 1.9 %copy.14 = bf16[512,512]{1,0:T(8,128)(2,1)} copy(bf16[512,512]{1,0:T(8,128)(2,1)} %shard_map.118) | data formatting | bytes 1048576
Async XLA Ops:
  0.0 0.7 copy-start

commit v4 on v3

--- a/solution.py
+++ b/solution.py
@@ -925,8 +925,8 @@
 
     @pl.when(inner)
     def _():
-        send_mat(1, far_straight, False)
-        send_mat(1, far_straight, True)
+        send_mat(1, far_straight[:1], False)
+        send_mat(1, far_straight[:1], True)
 
     ow_copy(2, landed=True).wait_recv()
     ow_pass().start()
@@ -1019,10 +1019,8 @@
 
     @pl.when(jnp.logical_not(inner))
     def _():
-        send_mat(1, far_straight, False)
-        send_mat(1, far_straight, True)
-
-    send_mat(1, (2,), True)
+        send_mat(1, far_straight[1:], False)
+        send_mat(1, far_straight[1:], True)
 
     def up_block(mm):
         def one(i, _):
@@ -1052,8 +1050,19 @@
     pass_on(((1, 0), (2, 0), (1, 1), (2, 1)))
     send_mat(1, [r for r in turning if r > 1], False)
     send_mat(1, (1,), False)
-    send_mat(1, (3,), True)
+    send_mat(1, (2, 3), True)
     send_up(1, far_straight)
+
+    @pl.when(inner)
+    def _():
+        send_mat(1, far_straight[1:], False)
+        send_mat(1, far_straight[1:], True)
+
+    @pl.when(jnp.logical_not(inner))
+    def _():
+        send_mat(1, far_straight[:1], False)
+        send_mat(1, far_straight[:1], True)
+
     for e in range(2):
         for h in range(2):
             t3_copy(0, h, e, landed=True).wait_recv()
@@ -1070,11 +1079,10 @@
                 t3_copy(r, h, e, landed=True).wait_recv()
         up_block(member(r))
 
-    def piece(mm, tq, fh):
-        rows = aligned((tq * (cols // block) + fh) * block, block)
+    def piece(mm, tq):
         return lax.dot_general(
             act[aligned(mm * tok, tok), :],
-            down[rows, :],
+            down[lanes_of(tq, cols), :],
             (((1,), (1,)), ((), ())),
             preferred_element_type=F32,
         )
@@ -1094,14 +1102,18 @@
             near_in.at[p, h, r],
             near_send.at[p, h, r],
             near_recv.at[p, h, r],
-            sp=group_dev(2 if r == 2 else 1),
-        )
+            sp=group_dev(r if r < 3 else lead(h)),
+        )
+
+    def lead(h):
+        return 1 if h else 2
 
     def near_on(p, h):
         near_copy(p, h, 3).wait_recv()
-        both = summed[p, h, member(2)].astype(F32) + near_in[p, h, 3].astype(F32)
-        summed[p, h, member(2)] = both.astype(BF16)
-        near_copy(p, h, 2).start()
+        rest = 3 - lead(h)
+        both = summed[p, h, member(rest)].astype(F32) + near_in[p, h, 3].astype(F32)
+        summed[p, h, member(rest)] = both.astype(BF16)
+        near_copy(p, h, rest).start()
 
     def side_copy(mm):
         return remote(side_out.at[mm], side_in.at[mm], side_send.at[mm], side_recv.at[mm], tp=across)
@@ -1118,19 +1130,16 @@
             w_copy(1, r, landed=True).wait_recv()
         for r in member_order:
             mm = member(r)
-            for fh in range(2):
-                pair_out[p, mm, :, pl.ds(fh * block, block)] = piece(
-                    mm, 2 * xp + 1 - c, fh
-                ).astype(BF16)
+            pair_out[p, mm] = piece(mm, 2 * xp + 1 - c).astype(BF16)
             pair_copy(p, mm).start()
         for r in member_order:
             mm = member(r)
             pair_copy(p, mm).wait_recv()
-            v = piece(mm, 2 * xp + c, 1) + pair_in[p, mm, :, pl.ds(block, block)].astype(F32)
-            summed[p, 1, mm] = v.astype(BF16)
+            both = piece(mm, 2 * xp + c) + pair_in[p, mm].astype(F32)
+            summed[p, 1, mm] = both[:, block:].astype(BF16)
             if r % 2:
                 near_copy(p, 1, r).start()
-            v = piece(mm, 2 * xp + c, 0) + pair_in[p, mm, :, pl.ds(0, block)].astype(F32)
+            v = both[:, :block]
 
             @pl.when(xp == x)
             def _():
@@ -1151,7 +1160,7 @@
                 side_copy(mm).wait_recv()
                 if r:
                     summed[p, 0, mm] = (held[p, mm] + side_in[mm].astype(F32)).astype(BF16)
-                if r % 2:
+                if r in (3, lead(0)):
                     near_copy(p, 0, r).start()
             if 0 in rs:
                 near_on(p, 0)

time: 173 us -> 171 us (0.988)
  no operation moved by 1% of the time
where the time goes in v4:
time: 171 us; the launch traced here: 169 us
  Pallas kernels  166 us (97%)
  local copies, waits for them, and re-layouts  2.55 us (1%)
    pallas_call x1, Pallas kernels, grouped_call(): pl.pallas_call(functools.partial(grouped_kernel, n, t), out_shape=jax.Sha...  166 us

profile of v4, /device:TPU:25, one launch (start us, length us, event | category | flops | bytes accessed | tf_op | source)
XLA Modules:
  0.0 169.4 jit_solution(4007223601245361957)
XLA Ops:
  0.0 0.0 copy-start
  0.0 0.7 copy-done
  0.7 0.6 pad_convert_fusion.br_in
  1.3 166.2 %shard_map.118 = bf16[512,512]{1,0:T(8,128)(2,1)} custom-call(bf16[512,256]{1,0:T(8,128)(2,1)} %q_in.1, bf16[512,256]{1,0:T(8,128)(2,1)} %k_in.1, bf16[512,256]{1,0:T(8,128)(2,1)} %v_in.1, f32[8,512]{1,0:T(8,128)} %pad_convert_fusion.br_in, bf16[512,512]{1,0:T(8,128)(2,1)} %res_in.1, bf16[256,2048]{1,0:T(8,128)(2,1)} %ow_in.1, f32[1,2048]{1,0:T(1,128)} %bitcast.5, ...), custom_call_target="tpu_custom_call" | custom-call | tf_op jit(solution)/shard_map/pallas_call | solution.py:1320
  167.5 1.9 %copy.14 = bf16[512,512]{1,0:T(8,128)(2,1)} copy(bf16[512,512]{1,0:T(8,128)(2,1)} %shard_map.118) | data formatting | bytes 1048576
Async XLA Ops:
  0.0 0.7 copy-start
